TPU v7x, 32 devices: a whole 2x2x4 slice. The times are simulated.
32 devices in a mesh: sp: 16 (over z, y, x), tp: 2 (over core).
Axes of the slice: x: 2, y: 2, z: 4, core: 2. Of those that a mesh axis runs over, the one named last changes fastest.
Arguments:
- value_in: bfloat16 [4096, 2048], P('sp', 'tp'), may hold values from -25 to 25, as said below
- gate_in: bfloat16 [4096, 2048], P('sp', 'tp'), may hold values from -6 to 6
- taps: float32 [31, 2048], P(None, 'tp'), may hold values from -1 to 1
- gain: float32 [2048], P('tp'), may hold values from 0.1 to 1.9
- shift: float32 [2048], P('tp'), may hold values from -3 to 3
- w_out: bfloat16 [2048, 2048], P('tp'), may hold values from -0.125 to 0.125
- grad_out: bfloat16 [4096, 2048], P('sp'), may hold values from -6 to 6
Outputs:
- d_value: bfloat16 [4096, 2048], P('sp', 'tp')
- d_gate: bfloat16 [4096, 2048], P('sp', 'tp')
- d_taps: float32 [31, 2048], P(None, 'tp')
- d_gain: float32 [2048], P('tp')
- d_shift: float32 [2048], P('tp')
Inputs may be any that keep to these rules, and one draw needn't show every extreme that they name: `value_in`: channel blocks of different magnitude.
All inputs are finite; a program needn't handle non-finite values.
Results may differ from a plain program's by a relative error of at most 0.007.
Values may be sent and summed in bfloat16 or wider, within the bound.
No kernel may reach another device: no remote copies, remote signals or barrier semaphores. Data moves between devices by JAX's collectives and lax.ppermute only.
A program may use at most 64 MiB of HBM per device.

v0:
```python
import math
import jax
import jax.numpy as jnp
from jax import lax
from jax.sharding import PartitionSpec as P

EPS = 1e-05


def with_halo(block, sides, width):
    for axis, dim in sides:
        count = lax.axis_size(axis)
        forward = [(i, i + 1) for i in range(count - 1)]
        backward = [(target, source) for source, target in forward]
        low = lax.ppermute(
            lax.slice_in_dim(block, block.shape[dim] - width, None, axis=dim), axis, forward
        )
        high = lax.ppermute(lax.slice_in_dim(block, 0, width, axis=dim), axis, backward)
        block = jnp.concatenate([low, block, high], axis=dim)
    return block


def gated_rows(value_rows, gate_rows):
    gate_sig = jax.nn.sigmoid(gate_rows.astype(jnp.float32))
    return ((value_rows.astype(jnp.float32) * gate_sig).astype(jnp.bfloat16), gate_sig)


def convolve(window, taps, count):
    wide = window.astype(jnp.float32)
    total = jnp.zeros((count, wide.shape[1]), jnp.float32)
    for offset in range(taps.shape[0]):
        total = total + taps[offset] * wide[offset : offset + count]
    return total


def norm_backward(conv_out, grad_rows, gain, shift, w_out, width):
    sums, squares = lax.psum((jnp.sum(conv_out, 1), jnp.sum(conv_out * conv_out, 1)), "tp")
    mean = sums / width
    var = squares / width - mean * mean
    inv = lax.rsqrt(var + EPS)
    normed = (conv_out - mean[:, None]) * inv[:, None]
    pre = normed * gain + shift
    grad_mix = lax.dot_general(
        grad_rows, w_out, (((1,), (1,)), ((), ())), preferred_element_type=jnp.float32
    )
    sig = jax.nn.sigmoid(pre)
    grad_pre = grad_mix * sig * (1.0 + pre * (1.0 - sig))
    grad_normed = grad_pre * gain
    first, second = lax.psum((jnp.sum(grad_normed, 1), jnp.sum(grad_normed * normed, 1)), "tp")
    grad_conv = inv[:, None] * (
        grad_normed - first[:, None] / width - normed * second[:, None] / width
    )
    return (grad_conv, grad_pre, normed)


def shards(value_in, gate_in, taps, gain, shift, w_out, grad_out):
    half = taps.shape[0] // 2
    kernel = taps.shape[0]
    rows = value_in.shape[0]
    width = value_in.shape[1] * lax.axis_size("tp")
    total = rows * lax.axis_size("sp")
    gated, gate_sig = gated_rows(value_in, gate_in)
    gated_wide = with_halo(gated, (("sp", 0),), half)
    conv_out = convolve(gated_wide, taps, rows)
    grad_conv, grad_pre, normed = norm_backward(conv_out, grad_out, gain, shift, w_out, width)
    grad_wide = with_halo(grad_conv, (("sp", 0),), half)
    own_grad = grad_wide[half : half + rows]
    gated_float = gated_wide.astype(jnp.float32)
    grad_gated = jnp.zeros((rows, own_grad.shape[1]), jnp.float32)
    for offset in range(kernel):
        grad_gated = (
            grad_gated + taps[offset] * grad_wide[2 * half - offset : 2 * half - offset + rows]
        )
    tap_terms = jnp.stack(
        [jnp.sum(own_grad * gated_float[offset : offset + rows], 0) for offset in range(kernel)]
    )
    scale = 1.0 / math.sqrt(total)
    stacked = (
        jnp.concatenate(
            [tap_terms, jnp.sum(grad_pre * normed, 0)[None], jnp.sum(grad_pre, 0)[None]], 0
        )
        * scale
    )
    summed = lax.psum(stacked, "sp")
    d_taps = summed[:kernel]
    d_gain = summed[kernel]
    d_shift = summed[kernel + 1]
    d_value = (grad_gated * gate_sig).astype(jnp.bfloat16)
    d_gate = (grad_gated * value_in.astype(jnp.float32) * gate_sig * (1.0 - gate_sig)).astype(
        jnp.bfloat16
    )
    return (d_value, d_gate, d_taps, d_gain, d_shift)


def solution(mesh):
    return jax.shard_map(
        shards,
        mesh=mesh,
        in_specs=(
            P("sp", "tp"),
            P("sp", "tp"),
            P(None, "tp"),
            P("tp"),
            P("tp"),
            P("tp", None),
            P("sp", None),
        ),
        out_specs=(P("sp", "tp"), P("sp", "tp"), P(None, "tp"), P("tp"), P("tp")),
        check_vma=False,
    )
```

profile of v0, /device:TPU:0, one launch (start us, length us, event | category | flops | bytes accessed | tf_op | source)
XLA Modules:
  0.0 175.2 jit_solution(298959568165321427)
XLA Ops:
  7.2 0.0 all-reduce.4.cloned.1.call-start
  7.2 1.6 fusion.1
  8.9 4.9 %collective-permute-start = (bf16[15,1024]{1,0:T(8,128)(2,1)S(1)}, bf16[15,1024]{1,0:T(8,128)(2,1)S(1)}, u32[]{:S(2)}, u32[]{:S(2)}) collective-permute-start(bf16[15,1024]{1,0:T(8,128)(2,1)S(1)} %get-tuple-element.52), channel_id=1, source_target_pairs={{0,2},{2,4},{4,6},{6,8},{8,10},{10,12},{12,14},{14,16},{16,18},{18... | collective-permute-start | bytes 92168 | tf_op jit(solution)/shard_map/ppermute | solution.py:15
  13.7 1.3 collective-permute-start.1
  15.0 0.1 fusion.97
  15.4 4.2 %collective-permute-done.1 = bf16[15,1024]{1,0:T(8,128)(2,1)S(1)} collective-permute-done((bf16[15,1024]{1,0:T(8,128)(2,1)S(1)}, bf16[15,1024]{1,0:T(8,128)(2,1)S(1)}, u32[]{:S(2)}, u32[]{:S(2)}) %collective-permute-start.1) | collective-permute-done | bytes 30752 | tf_op jit(solution)/shard_map/ppermute | solution.py:18
  19.5 0.2 maximum_convert_fusion
  19.7 5.7 %multiply_reduce_fusion.33 = (f32[256]{0:T(256)S(1)}, f32[256]{0:T(256)S(1)}, f32[256,1024]{1,0:T(8,128)S(1)}) fusion(f32[286,1024]{1,0:T(8,128)S(1)} %maximum_convert_fusion, f32[1024]{0:T(1024)S(1)} %bitcast.126, f32[1024]{0:T(1024)S(1)} %bitcast.128, f32[1024]{0:T(1024)S(1)} %bitcast.70, f32[1024]{0:T(1024)S(1)} %bitcast.72, f32[1024]{0:T(1024)S(1)} %bitcast.74, ...), kind=kLoop, calls=%fused_computation.186 | loop fusion | flops 16776704 | bytes 33683456 | tf_op jit(solution)/shard_map/reduce_sum | solution.py:37
  25.6 2.5 %all-reduce.1 = (f32[256]{0:T(256)S(1)}, f32[256]{0:T(256)S(1)}) all-reduce(f32[256]{0:T(256)S(1)} %get-tuple-element.41, f32[256]{0:T(256)S(1)} %get-tuple-element.40), channel_id=1, replica_groups=mesh['sp'=16,'tp'=2] {'tp'}, use_global_device_ids=true, to_apply=%region_3.0 | all-reduce | flops 512 | bytes 4096 | tf_op jit(solution)/shard_map/psum | solution.py:37
  28.1 5.5 %multiply_reduce_fusion = (f32[1024]{0:T(1024)}, f32[256]{0:T(256)S(1)}, f32[256]{0:T(256)S(1)}, f32[1024]{0:T(1024)}, f32[256,1024]{1,0:T(8,128)}) fusion(f32[256,1024]{1,0:T(8,128)S(1)} %get-tuple-element.49, f32[256]{0:T(256)S(1)} %get-tuple-element.88, f32[256]{0:T(256)S(1)} %get-tuple-element.87, f32[1024]{0:T(1024)S(1)} %copy-done.24, ...), kind=kOutput, calls=%fused_computation.150 | convolution fusion | flops 1078720000 | bytes 7360512 | tf_op jit(solution)/shard_map/dot_general | solution.py:43
  33.7 2.4 %all-reduce = (f32[256]{0:T(256)S(1)}, f32[256]{0:T(256)S(1)}) all-reduce(f32[256]{0:T(256)S(1)} %get-tuple-element.37, f32[256]{0:T(256)S(1)} %get-tuple-element.38), channel_id=1, replica_groups=mesh['sp'=16,'tp'=2] {'tp'}, use_global_device_ids=true, to_apply=%region_7.0 | all-reduce | flops 512 | bytes 4096 | tf_op jit(solution)/shard_map/psum | solution.py:49
  36.1 4.8 %multiply_reduce_fusion.1 = (f32[1024]{0:T(1024)}, f32[1024]{0:T(1024)}, f32[1024]{0:T(1024)}, f32[1024]{0:T(1024)}, f32[1024]{0:T(1024)}, /*index=5*/f32[1024]{...) fusion(f32[286,1024]{1,0:T(8,128)S(1)} %maximum_convert_fusion,, ...), kind=kLoop, calls=%fused_computation.151 | loop fusion | flops 11515904 | bytes 22102016 | tf_op jit(solution)/shard_map/reduce_sum | solution.py:75
  41.0 2.4 %multiply_reduce_fusion.2 = (f32[1024]{0:T(1024)}, f32[1024]{0:T(1024)}, f32[1024]{0:T(1024)}, f32[1024]{0:T(1024)}, f32[1024]{0:T(1024)}, /*index=5*/f32[1024]{...) fusion(f32[256,1024]{1,0:T(8,128)S(1)} %get-tuple-element.46, ...), kind=kLoop, calls=%fused_computation.152 | loop fusion | flops 6802432 | bytes 14733312 | tf_op jit(solution)/shard_map/reduce_sum | solution.py:75
  43.3 0.6 fusion.94
  44.0 1.3 collective-permute-start.2
  45.3 4.9 %collective-permute-start.3 = (f32[15,1024]{1,0:T(8,128)S(1)}, f32[15,1024]{1,0:T(8,128)S(1)}, u32[]{:S(2)}, u32[]{:S(2)}) collective-permute-start(f32[15,1024]{1,0:T(8,128)S(1)} %get-tuple-element.51), channel_id=1, source_target_pairs={{0,2},{2,4},{4,6},{6,8},{8,10},{10,12},{12,14},{14,16},{16,18},{18... | collective-permute-start | bytes 184328 | tf_op jit(solution)/shard_map/ppermute | solution.py:15
  50.2 3.8 %concatenate.44 = f32[33,1024]{1,0:T(8,128)S(1)} concatenate(f32[1,1024]{1,0:T(1,128)} %bitcast.160, f32[1,1024]{1,0:T(1,128)} %bitcast.159, f32[1,1024]{1,0:T(1,128)} %bitcast.158, f32[1,1024]{1,0:T(1,128)} %bitcast.157, f32[1,1024]{1,0:T(1,128)} %bitcast.156, f32[1,1024]{1,0:T(1,128)} %bitcast.155, f32[1,1024]{1,0:T(1,128)} %bitcast.154, f32[1,1024]{1,0:T(1,128)} %bitcast.153, ...), dimensions={0} | concatenate | bytes 270336 | tf_op jit(solution)/shard_map/concatenate | solution.py:79
  54.0 0.7 broadcast_multiply_fusion
  54.7 0.0 all-reduce.4.cloned.1.call-update
  54.8 6.9 %fusion.4 = (bf16[256,1024]{1,0:T(8,128)(2,1)}, f32[256,1024]{1,0:T(8,128)}) fusion(bf16[256,1024]{1,0:T(8,128)(2,1)S(1)} %copy-done.3, bf16[256,1024]{1,0:T(8,128)(2,1)S(1)} %copy-done.1, f32[256,1024]{1,0:T(8,128)S(1)} %get-tuple-element.46, f32[15,1024]{1,0:T(8,128)S(1)} %collective-permute-done.3, f32[1024]{0:T(1024)} %bitcast.127, f32[1024]{0:T(1024)} %bitcast.129, ...), kind=kLoop, calls=%fused_computation.35 | loop fusion | flops 26476544 | bytes 3919872 | tf_op jit(solution)/shard_map/convert_element_type | solution.py:89
  61.7 2.3 %multiply_convert_fusion = bf16[256,1024]{1,0:T(8,128)(2,1)} fusion(f32[256,1024]{1,0:T(8,128)} %get-tuple-element.48, bf16[256,1024]{1,0:T(8,128)(2,1)S(1)} %copy-done.1), kind=kLoop, calls=%fused_computation.182 | loop fusion | flops 1572864 | bytes 2097152 | tf_op jit(solution)/shard_map/convert_element_type | solution.py:88
  64.0 101.4 %all-reduce.4.cloned.1.call-done = f32[33,1024]{1,0:T(8,128)} async-done(((f32[33,1024]{1,0:T(8,128)}), f32[33,1024]{1,0:T(8,128)}) %all-reduce.4.cloned.1.call-update) | async-done | bytes 135184 | tf_op jit(solution)/shard_map/psum | solution.py:84
  165.4 1.4 fusion.96
  166.8 1.6 slice.579
  (59 shorter events, 0.2 us)
Async XLA Ops:
  7.2 20.9 %copy-start = (bf16[256,2048]{1,0:T(8,128)(2,1)S(1)}, bf16[256,2048]{1,0:T(8,128)(2,1)}, u32[]{:S(2)}) copy-start(bf16[256,2048]{1,0:T(8,128)(2,1)} %param.13) | copy-start | bytes 3145732
  7.2 158.2 %all-reduce.4.cloned.1.call-start = ((), (), s32[]{:S(2)}) async-start(), calls=%async_computation | async-start | bytes 327680 | tf_op jit(solution)/shard_map/psum | solution.py:84
  8.9 6.5 %collective-permute-start = (bf16[15,1024]{1,0:T(8,128)(2,1)S(1)}, bf16[15,1024]{1,0:T(8,128)(2,1)S(1)}, u32[]{:S(2)}, u32[]{:S(2)}) collective-permute-start(bf16[15,1024]{1,0:T(8,128)(2,1)S(1)} %get-tuple-element.52), channel_id=1, source_target_pairs={{0,2},{2,4},{4,6},{6,8},{8,10},{10,12},{12,14},{14,16},{16,18},{18... | collective-permute-start | bytes 92168 | tf_op jit(solution)/shard_map/ppermute | solution.py:15
  13.7 5.8 %collective-permute-start.1 = (bf16[15,1024]{1,0:T(8,128)(2,1)S(1)}, bf16[15,1024]{1,0:T(8,128)(2,1)S(1)}, u32[]{:S(2)}, u32[]{:S(2)}) collective-permute-start(bf16[15,1024]{1,0:T(8,128)(2,1)S(1)} %get-tuple-element.53), channel_id=1, source_target_pairs={{2,0},{4,2},{6,4},{8,6},{10,8},{12,10},{14,12},{16,14},{18,16},{20... | collective-permute-start | bytes 92168 | tf_op jit(solution)/shard_map/ppermute | solution.py:18
  15.1 10.3 %copy-start.5 = (f32[1,1024]{1,0:T(1,128)}, f32[1,1024]{1,0:T(1,128)S(1)}, u32[]{:S(2)}) copy-start(f32[1,1024]{1,0:T(1,128)S(1)} %get-tuple-element.68) | copy-start | bytes 12292
  15.1 10.3 %copy-start.6 = (f32[1,1024]{1,0:T(1,128)}, f32[1,1024]{1,0:T(1,128)S(1)}, u32[]{:S(2)}) copy-start(f32[1,1024]{1,0:T(1,128)S(1)} %get-tuple-element.69) | copy-start | bytes 12292
  15.1 10.3 %copy-start.7 = (f32[1,1024]{1,0:T(1,128)}, f32[1,1024]{1,0:T(1,128)S(1)}, u32[]{:S(2)}) copy-start(f32[1,1024]{1,0:T(1,128)S(1)} %get-tuple-element.70) | copy-start | bytes 12292
  15.1 10.3 %copy-start.8 = (f32[1,1024]{1,0:T(1,128)}, f32[1,1024]{1,0:T(1,128)S(1)}, u32[]{:S(2)}) copy-start(f32[1,1024]{1,0:T(1,128)S(1)} %get-tuple-element.71) | copy-start | bytes 12292
  15.1 10.3 %copy-start.9 = (f32[1,1024]{1,0:T(1,128)}, f32[1,1024]{1,0:T(1,128)S(1)}, u32[]{:S(2)}) copy-start(f32[1,1024]{1,0:T(1,128)S(1)} %get-tuple-element.72) | copy-start | bytes 12292
  15.2 10.3 %copy-start.10 = (f32[1,1024]{1,0:T(1,128)}, f32[1,1024]{1,0:T(1,128)S(1)}, u32[]{:S(2)}) copy-start(f32[1,1024]{1,0:T(1,128)S(1)} %get-tuple-element.73) | copy-start | bytes 12292
  15.2 10.3 %copy-start.11 = (f32[1,1024]{1,0:T(1,128)}, f32[1,1024]{1,0:T(1,128)S(1)}, u32[]{:S(2)}) copy-start(f32[1,1024]{1,0:T(1,128)S(1)} %get-tuple-element.74) | copy-start | bytes 12292
  15.2 10.3 %copy-start.12 = (f32[1,1024]{1,0:T(1,128)}, f32[1,1024]{1,0:T(1,128)S(1)}, u32[]{:S(2)}) copy-start(f32[1,1024]{1,0:T(1,128)S(1)} %get-tuple-element.75) | copy-start | bytes 12292
  15.2 10.3 %copy-start.13 = (f32[1,1024]{1,0:T(1,128)}, f32[1,1024]{1,0:T(1,128)S(1)}, u32[]{:S(2)}) copy-start(f32[1,1024]{1,0:T(1,128)S(1)} %get-tuple-element.76) | copy-start | bytes 12292
  15.2 10.3 %copy-start.14 = (f32[1,1024]{1,0:T(1,128)}, f32[1,1024]{1,0:T(1,128)S(1)}, u32[]{:S(2)}) copy-start(f32[1,1024]{1,0:T(1,128)S(1)} %get-tuple-element.77) | copy-start | bytes 12292
  15.3 10.3 %copy-start.15 = (f32[1,1024]{1,0:T(1,128)}, f32[1,1024]{1,0:T(1,128)S(1)}, u32[]{:S(2)}) copy-start(f32[1,1024]{1,0:T(1,128)S(1)} %get-tuple-element.78) | copy-start | bytes 12292
  15.3 10.3 %copy-start.16 = (f32[1,1024]{1,0:T(1,128)}, f32[1,1024]{1,0:T(1,128)S(1)}, u32[]{:S(2)}) copy-start(f32[1,1024]{1,0:T(1,128)S(1)} %get-tuple-element.79) | copy-start | bytes 12292
  15.3 10.3 %copy-start.17 = (f32[1,1024]{1,0:T(1,128)}, f32[1,1024]{1,0:T(1,128)S(1)}, u32[]{:S(2)}) copy-start(f32[1,1024]{1,0:T(1,128)S(1)} %get-tuple-element.80) | copy-start | bytes 12292
  15.3 10.3 %copy-start.18 = (f32[1,1024]{1,0:T(1,128)}, f32[1,1024]{1,0:T(1,128)S(1)}, u32[]{:S(2)}) copy-start(f32[1,1024]{1,0:T(1,128)S(1)} %get-tuple-element.81) | copy-start | bytes 12292
  15.3 10.3 %copy-start.19 = (f32[1,1024]{1,0:T(1,128)}, f32[1,1024]{1,0:T(1,128)S(1)}, u32[]{:S(2)}) copy-start(f32[1,1024]{1,0:T(1,128)S(1)} %get-tuple-element.82) | copy-start | bytes 12292
  15.3 10.3 %copy-start.20 = (f32[1,1024]{1,0:T(1,128)}, f32[1,1024]{1,0:T(1,128)S(1)}, u32[]{:S(2)}) copy-start(f32[1,1024]{1,0:T(1,128)S(1)} %get-tuple-element.83) | copy-start | bytes 12292
  43.3 11.4 %copy-start.1 = (bf16[256,1024]{1,0:T(8,128)(2,1)S(1)}, bf16[256,1024]{1,0:T(8,128)(2,1)}, u32[]{:S(2)}) copy-start(bf16[256,1024]{1,0:T(8,128)(2,1)} %param.8) | copy-start | bytes 1572868
  43.3 11.4 %copy-start.3 = (bf16[256,1024]{1,0:T(8,128)(2,1)S(1)}, bf16[256,1024]{1,0:T(8,128)(2,1)}, u32[]{:S(2)}) copy-start(bf16[256,1024]{1,0:T(8,128)(2,1)} %param.7) | copy-start | bytes 1572868
  44.0 10.7 %collective-permute-start.2 = (f32[15,1024]{1,0:T(8,128)}, f32[15,1024]{1,0:T(8,128)S(1)}, u32[]{:S(2)}, u32[]{:S(2)}) collective-permute-start(f32[15,1024]{1,0:T(8,128)} %get-tuple-element.50), channel_id=1, source_target_pairs={{2,0},{4,2},{6,4},{8,6},{10,8},{12,10},{14,12},{16,14},{18,16},{20... | collective-permute-start | bytes 184328 | tf_op jit(solution)/shard_map/ppermute | solution.py:18
  45.3 9.5 %collective-permute-start.3 = (f32[15,1024]{1,0:T(8,128)S(1)}, f32[15,1024]{1,0:T(8,128)S(1)}, u32[]{:S(2)}, u32[]{:S(2)}) collective-permute-start(f32[15,1024]{1,0:T(8,128)S(1)} %get-tuple-element.51), channel_id=1, source_target_pairs={{0,2},{2,4},{4,6},{6,8},{8,10},{10,12},{12,14},{14,16},{16,18},{18... | collective-permute-start | bytes 184328 | tf_op jit(solution)/shard_map/ppermute | solution.py:15
  (7 other events, 63.5 us)
Sparse Core Ops, SparseCore 0:
  54.8 110.4 all-reduce.3
where the time goes:
time: 176 us; the launch traced here: 175 us
  waiting for transfers between devices  106 us (60%)
  other arithmetic  24.5 us (14%)
  between operations  14.5 us (8%)
  starting transfers between devices  12.4 us (7%)
  local copies, waits for them, and re-layouts  7.63 us (4%)
  matrix products  5.53 us (3%)
  blocking collectives  4.91 us (3%)
    psum x1, waiting for transfers between devices, shards(): summed = lax.psum(stacked, 'sp')  101 us
    ppermute x2, starting transfers between devices, with_halo(): lax.ppermute(lax.slice_in_dim(block, block.shape[dim] - width, None, axis...  9.8 us
    reduce_sum x2, other arithmetic, shards(): jnp.sum(own_grad * gated_float[offset:offset + rows], 0)  7.23 us
    convert_element_type x1, other arithmetic, shards(): (grad_gated * value_in.astype(jnp.float32) * gate_sig * (1.0 - gate_sig))...  6.89 us
    reduce_sum x1, other arithmetic, norm_backward(): jnp.sum(conv_out * conv_out, 1)  5.69 us
    dot_general x1, matrix products, norm_backward(): lax.dot_general(grad_rows, w_out, (((1,), (1,)), ((), ())), preferred_ele...  5.53 us
    ppermute x2, waiting for transfers between devices, with_halo(): lax.ppermute(lax.slice_in_dim(block, 0, width, axis=dim), axis, backward)  4.19 us
    concatenate x1, local copies, waits for them, and re-layouts, shards(): jnp.concatenate([tap_terms, jnp.sum(grad_pre * normed, 0)[None], jnp.sum(...  3.82 us
  transfers between devices with their start and end apart: 5, of which 2 were waited for; matrix products, arithmetic and copies ran while one was open for 8% of the time, Pallas kernels for 0%

commit v1 on v0

--- a/solution.py
+++ b/solution.py
@@ -81,7 +81,7 @@
         )
         * scale
     )
-    summed = lax.psum(stacked, "sp")
+    summed = jnp.sum(lax.all_gather(stacked, "sp"), axis=0)
     d_taps = summed[:kernel]
     d_gain = summed[kernel]
     d_shift = summed[kernel + 1]

time: 176 us -> 122 us (0.69)
  waiting for transfers between devices: 106 us -> 56.2 us
  local copies, waits for them, and re-layouts: 7.63 us -> 3.83 us
    psum x1 -> x0, waiting for transfers between devices: 101 us -> none  [shards(): summed = lax.psum(stacked, 'sp')]
    all_gather x0 -> x1, waiting for transfers between devices: none -> 48.6 us  [shards(): summed = jnp.sum(lax.all_gather(stacked, 'sp'), axis=0)]
    ppermute x2, waiting for transfers between devices: 0.01 us -> 2.88 us  [with_halo(): lax.ppermute(lax.slice_in_dim(block, block.shape[dim] - width, None, axis...]
    reduce_sum x0 -> x1, other arithmetic: none -> 1.92 us  [shards(): summed = jnp.sum(lax.all_gather(stacked, 'sp'), axis=0)]
  transfers between devices with their start and end apart: 5 -> 5, of which waited for: 2 -> 5; matrix products, arithmetic and copies ran while one was open for 8% -> 7% of each run, Pallas kernels for 0% -> 0%
where the time goes in v1:
time: 122 us
  waiting for transfers between devices  56.2 us (46%)
  other arithmetic  24.7 us (20%)
  between operations  14.2 us (12%)
  starting transfers between devices  12.4 us (10%)
  matrix products  5.52 us (5%)
  blocking collectives  4.91 us (4%)
  local copies, waits for them, and re-layouts  3.83 us (3%)
    all_gather x1, waiting for transfers between devices, shards(): summed = jnp.sum(lax.all_gather(stacked, 'sp'), axis=0)  48.6 us
    ppermute x2, starting transfers between devices, with_halo(): lax.ppermute(lax.slice_in_dim(block, block.shape[dim] - width, None, axis...  9.8 us
    reduce_sum x2, other arithmetic, shards(): jnp.sum(own_grad * gated_float[offset:offset + rows], 0)  6.57 us
    convert_element_type x1, other arithmetic, shards(): (grad_gated * value_in.astype(jnp.float32) * gate_sig * (1.0 - gate_sig))...  5.81 us
    reduce_sum x1, other arithmetic, norm_backward(): jnp.sum(conv_out * conv_out, 1)  5.69 us
    dot_general x1, matrix products, norm_backward(): lax.dot_general(grad_rows, w_out, (((1,), (1,)), ((), ())), preferred_ele...  5.52 us
    ppermute x2, waiting for transfers between devices, with_halo(): lax.ppermute(lax.slice_in_dim(block, 0, width, axis=dim), axis, backward)  4.71 us
    ppermute x2, waiting for transfers between devices, with_halo(): lax.ppermute(lax.slice_in_dim(block, block.shape[dim] - width, None, axis...  2.88 us
  transfers between devices with their start and end apart: 5, of which 5 were waited for; matrix products, arithmetic and copies ran while one was open for 7% of the time, Pallas kernels for 0%

profile of v1, /device:TPU:0, one launch (start us, length us, event | category | flops | bytes accessed | tf_op | source)
XLA Modules:
  0.0 121.8 jit_solution(4767323120637284882)
XLA Ops:
  7.2 1.6 %fusion.1 = bf16[256,1024]{1,0:T(8,128)(2,1)S(1)} fusion(bf16[256,1024]{1,0:T(8,128)(2,1)} %param.7, bf16[256,1024]{1,0:T(8,128)(2,1)} %param.8), kind=kLoop, calls=%fused_computation.32 | loop fusion | flops 1835008 | bytes 1572864 | tf_op jit(solution)/shard_map/convert_element_type | solution.py:25
  8.9 4.9 %collective-permute-start = (bf16[15,1024]{1,0:T(8,128)(2,1)S(1)}, bf16[15,1024]{1,0:T(8,128)(2,1)S(1)}, u32[]{:S(2)}, u32[]{:S(2)}) collective-permute-start(bf16[15,1024]{1,0:T(8,128)(2,1)S(1)} %get-tuple-element.52), channel_id=1, source_target_pairs={{0,2},{2,4},{4,6},{6,8},{8,10},{10,12},{12,14},{14,16},{16,18},{18... | collective-permute-start | bytes 92168 | tf_op jit(solution)/shard_map/ppermute | solution.py:15
  13.7 1.3 %collective-permute-start.1 = (bf16[15,1024]{1,0:T(8,128)(2,1)S(1)}, bf16[15,1024]{1,0:T(8,128)(2,1)S(1)}, u32[]{:S(2)}, u32[]{:S(2)}) collective-permute-start(bf16[15,1024]{1,0:T(8,128)(2,1)S(1)} %get-tuple-element.53), channel_id=1, source_target_pairs={{2,0},{4,2},{6,4},{8,6},{10,8},{12,10},{14,12},{16,14},{18,16},{20... | collective-permute-start | bytes 92168 | tf_op jit(solution)/shard_map/ppermute | solution.py:18
  15.2 0.2 collective-permute-done
  15.3 4.2 %collective-permute-done.1 = bf16[15,1024]{1,0:T(8,128)(2,1)S(1)} collective-permute-done((bf16[15,1024]{1,0:T(8,128)(2,1)S(1)}, bf16[15,1024]{1,0:T(8,128)(2,1)S(1)}, u32[]{:S(2)}, u32[]{:S(2)}) %collective-permute-start.1) | collective-permute-done | bytes 30752 | tf_op jit(solution)/shard_map/ppermute | solution.py:18
  19.5 0.2 maximum_convert_fusion
  19.7 5.7 %multiply_reduce_fusion.33 = (f32[256]{0:T(256)S(1)}, f32[256]{0:T(256)S(1)}, f32[256,1024]{1,0:T(8,128)S(1)}) fusion(f32[286,1024]{1,0:T(8,128)S(1)} %maximum_convert_fusion, f32[1024]{0:T(1024)S(1)} %bitcast.126, f32[1024]{0:T(1024)S(1)} %bitcast.128, f32[1024]{0:T(1024)S(1)} %bitcast.70, f32[1024]{0:T(1024)S(1)} %bitcast.72, f32[1024]{0:T(1024)S(1)} %bitcast.74, ...), kind=kLoop, calls=%fused_computation.186 | loop fusion | flops 16776704 | bytes 33683456 | tf_op jit(solution)/shard_map/reduce_sum | solution.py:37
  25.4 2.5 %all-reduce.1 = (f32[256]{0:T(256)S(1)}, f32[256]{0:T(256)S(1)}) all-reduce(f32[256]{0:T(256)S(1)} %get-tuple-element.41, f32[256]{0:T(256)S(1)} %get-tuple-element.40), channel_id=1, replica_groups=mesh['sp'=16,'tp'=2] {'tp'}, use_global_device_ids=true, to_apply=%region_3.0 | all-reduce | flops 512 | bytes 4096 | tf_op jit(solution)/shard_map/psum | solution.py:37
  27.9 5.5 %multiply_reduce_fusion = (f32[1024]{0:T(1024)}, f32[256]{0:T(256)S(1)}, f32[256]{0:T(256)S(1)}, f32[1024]{0:T(1024)}, f32[256,1024]{1,0:T(8,128)}) fusion(f32[256,1024]{1,0:T(8,128)S(1)} %get-tuple-element.49, f32[256]{0:T(256)S(1)} %get-tuple-element.88, f32[256]{0:T(256)S(1)} %get-tuple-element.87, f32[1024]{0:T(1024)S(1)} %copy-done.5, ...), kind=kOutput, calls=%fused_computation.150 | convolution fusion | flops 1078720000 | bytes 7360512 | tf_op jit(solution)/shard_map/dot_general | solution.py:43
  33.5 2.4 %all-reduce = (f32[256]{0:T(256)S(1)}, f32[256]{0:T(256)S(1)}) all-reduce(f32[256]{0:T(256)S(1)} %get-tuple-element.37, f32[256]{0:T(256)S(1)} %get-tuple-element.38), channel_id=1, replica_groups=mesh['sp'=16,'tp'=2] {'tp'}, use_global_device_ids=true, to_apply=%region_7.0 | all-reduce | flops 512 | bytes 4096 | tf_op jit(solution)/shard_map/psum | solution.py:49
  35.9 4.2 %multiply_reduce_fusion.1 = (f32[1024]{0:T(1024)S(1)}, f32[1024]{0:T(1024)S(1)}, f32[1024]{0:T(1024)S(1)}, f32[1024]{0:T(1024)S(1)}, f32[1024]{0:T(1024)S(1)}, /...) fusion(f32[286,1024]{1,0:T(8,128)S(1)} %maximum_convert_fusion,, ...), kind=kLoop, calls=%fused_computation.151 | loop fusion | flops 11515904 | bytes 22102016 | tf_op jit(solution)/shard_map/reduce_sum | solution.py:75
  40.1 2.4 %multiply_reduce_fusion.2 = (f32[1024]{0:T(1024)S(1)}, f32[1024]{0:T(1024)S(1)}, f32[1024]{0:T(1024)S(1)}, f32[1024]{0:T(1024)S(1)}, f32[1024]{0:T(1024)S(1)}, /...) fusion(f32[256,1024]{1,0:T(8,128)S(1)} %get-tuple-element.46, ...), kind=kLoop, calls=%fused_computation.152 | loop fusion | flops 6802432 | bytes 14733312 | tf_op jit(solution)/shard_map/reduce_sum | solution.py:75
  42.5 2.4 %concatenate.150 = f32[1,33,1024]{2,1,0:T(8,128)S(1)} concatenate(f32[1,1,1024]{2,1,0:T(1,128)} %bitcast.160, f32[1,1,1024]{2,1,0:T(1,128)} %bitcast.159, f32[1,1,1024]{2,1,0:T(1,128)S(1)} %bitcast.158, f32[1,1,1024]{2,1,0:T(1,128)S(1)} %bitcast.157, f32[1,1,1024]{2,1,0:T(1,128)S(1)} %bitcast.156, f32[1,1,1024]{2,1,0:T(1,128)S(1)} %bitcast.155, f32[1,1,1024]{2,1,0:T(1,128)S(1)} %bitcast.154, ...), dimensions={1} | concatenate | bytes 270336 | tf_op jit(solution)/shard_map/concatenate | solution.py:79
  44.9 0.7 broadcast_multiply_fusion
  45.6 1.3 %collective-permute-start.2 = (f32[15,1024]{1,0:T(8,128)S(1)}, f32[15,1024]{1,0:T(8,128)S(1)}, u32[]{:S(2)}, u32[]{:S(2)}) collective-permute-start(f32[15,1024]{1,0:T(8,128)S(1)} %get-tuple-element.50), channel_id=1, source_target_pairs={{2,0},{4,2},{6,4},{8,6},{10,8},{12,10},{14,12},{16,14},{18,16},{20... | collective-permute-start | bytes 184328 | tf_op jit(solution)/shard_map/ppermute | solution.py:18
  46.9 4.9 %collective-permute-start.3 = (f32[15,1024]{1,0:T(8,128)S(1)}, f32[15,1024]{1,0:T(8,128)S(1)}, u32[]{:S(2)}, u32[]{:S(2)}) collective-permute-start(f32[15,1024]{1,0:T(8,128)S(1)} %get-tuple-element.51), channel_id=1, source_target_pairs={{0,2},{2,4},{4,6},{6,8},{8,10},{10,12},{12,14},{14,16},{16,18},{18... | collective-permute-start | bytes 184328 | tf_op jit(solution)/shard_map/ppermute | solution.py:15
  51.8 0.5 collective-permute-done.2
  52.3 2.7 %collective-permute-done.3 = f32[15,1024]{1,0:T(8,128)S(1)} collective-permute-done((f32[15,1024]{1,0:T(8,128)S(1)}, f32[15,1024]{1,0:T(8,128)S(1)}, u32[]{:S(2)}, u32[]{:S(2)}) %collective-permute-start.3) | collective-permute-done | bytes 61472 | tf_op jit(solution)/shard_map/ppermute | solution.py:15
  55.0 5.8 %fusion.4 = (bf16[256,1024]{1,0:T(8,128)(2,1)}, f32[256,1024]{1,0:T(8,128)}) fusion(bf16[256,1024]{1,0:T(8,128)(2,1)S(1)} %copy-done.3, bf16[256,1024]{1,0:T(8,128)(2,1)S(1)} %copy-done.1, f32[256,1024]{1,0:T(8,128)S(1)} %get-tuple-element.46, f32[15,1024]{1,0:T(8,128)S(1)} %collective-permute-done.3, f32[1024]{0:T(1024)S(1)} %bitcast.127, ...), kind=kLoop, calls=%fused_computation.35 | loop fusion | flops 26476544 | bytes 3919872 | tf_op jit(solution)/shard_map/convert_element_type | solution.py:89
  60.9 2.3 %multiply_convert_fusion = bf16[256,1024]{1,0:T(8,128)(2,1)} fusion(f32[256,1024]{1,0:T(8,128)} %get-tuple-element.48, bf16[256,1024]{1,0:T(8,128)(2,1)S(1)} %copy-done.1), kind=kLoop, calls=%fused_computation.182 | loop fusion | flops 1572864 | bytes 2097152 | tf_op jit(solution)/shard_map/convert_element_type | solution.py:88
  63.2 48.6 %all-gather.2.cloned.1.call-done = f32[16,33,1024]{2,1,0:T(8,128)} async-done(((f32[1,33,1024]{2,1,0:T(8,128)}), f32[16,33,1024]{2,1,0:T(8,128)}) %all-gather.2.cloned.1.call-update) | async-done | bytes 2162704 | tf_op jit(solution)/shard_map/all_gather | solution.py:84
  111.8 1.9 %reduce_sum.379 = f32[33,1024]{1,0:T(8,128)S(1)} reduce(f32[16,33,1024]{2,1,0:T(8,128)} %all-gather.2.cloned.1.call-done, f32[]{:T(128)} %constant.6.clone.1), dimensions={0}, to_apply=%region_41.0 | reduce | flops 506880 | bytes 2297860 | tf_op jit(solution)/shard_map/reduce_sum | solution.py:84
  113.7 0.6 fusion.96
  114.3 0.7 slice.579
  (22 shorter events, 0.2 us)
Async XLA Ops:
  7.2 20.8 %copy-start = (bf16[256,2048]{1,0:T(8,128)(2,1)S(1)}, bf16[256,2048]{1,0:T(8,128)(2,1)}, u32[]{:S(2)}) copy-start(bf16[256,2048]{1,0:T(8,128)(2,1)} %param.13) | copy-start | bytes 3145732
  7.2 7.9 %copy-start.4 = (f32[31,1024]{1,0:T(8,128)S(1)}, f32[31,1024]{1,0:T(8,128)}, u32[]{:S(2)}) copy-start(f32[31,1024]{1,0:T(8,128)} %param.9) | copy-start | bytes 380932
  7.2 104.6 %all-gather.2.cloned.1.call-start = ((), (), s32[]{:S(2)}) async-start(), calls=%async_computation | async-start | bytes 2785280 | tf_op jit(solution)/shard_map/all_gather | solution.py:84
  8.9 6.5 %collective-permute-start = (bf16[15,1024]{1,0:T(8,128)(2,1)S(1)}, bf16[15,1024]{1,0:T(8,128)(2,1)S(1)}, u32[]{:S(2)}, u32[]{:S(2)}) collective-permute-start(bf16[15,1024]{1,0:T(8,128)(2,1)S(1)} %get-tuple-element.52), channel_id=1, source_target_pairs={{0,2},{2,4},{4,6},{6,8},{8,10},{10,12},{12,14},{14,16},{16,18},{18... | collective-permute-start | bytes 92168 | tf_op jit(solution)/shard_map/ppermute | solution.py:15
  13.7 5.8 %collective-permute-start.1 = (bf16[15,1024]{1,0:T(8,128)(2,1)S(1)}, bf16[15,1024]{1,0:T(8,128)(2,1)S(1)}, u32[]{:S(2)}, u32[]{:S(2)}) collective-permute-start(bf16[15,1024]{1,0:T(8,128)(2,1)S(1)} %get-tuple-element.53), channel_id=1, source_target_pairs={{2,0},{4,2},{6,4},{8,6},{10,8},{12,10},{14,12},{16,14},{18,16},{20... | collective-permute-start | bytes 92168 | tf_op jit(solution)/shard_map/ppermute | solution.py:18
  19.7 8.2 %copy-start.5 = (f32[1024]{0:T(1024)S(1)}, f32[1024]{0:T(1024)}, u32[]{:S(2)}) copy-start(f32[1024]{0:T(1024)} %param.10) | copy-start | bytes 12292
  19.7 8.2 %copy-start.6 = (f32[1024]{0:T(1024)S(1)}, f32[1024]{0:T(1024)}, u32[]{:S(2)}) copy-start(f32[1024]{0:T(1024)} %param.11) | copy-start | bytes 12292
  25.4 8.0 %copy-start.2 = (f32[256,1024]{1,0:T(8,128)}, f32[256,1024]{1,0:T(8,128)S(1)}, u32[]{:S(2)}) copy-start(f32[256,1024]{1,0:T(8,128)S(1)} %get-tuple-element.49) | copy-start | bytes 3145732
  42.5 12.6 %copy-start.1 = (bf16[256,1024]{1,0:T(8,128)(2,1)S(1)}, bf16[256,1024]{1,0:T(8,128)(2,1)}, u32[]{:S(2)}) copy-start(bf16[256,1024]{1,0:T(8,128)(2,1)} %param.8) | copy-start | bytes 1572868
  42.5 12.6 %copy-start.3 = (bf16[256,1024]{1,0:T(8,128)(2,1)S(1)}, bf16[256,1024]{1,0:T(8,128)(2,1)}, u32[]{:S(2)}) copy-start(bf16[256,1024]{1,0:T(8,128)(2,1)} %param.7) | copy-start | bytes 1572868
  45.6 6.7 %collective-permute-start.2 = (f32[15,1024]{1,0:T(8,128)S(1)}, f32[15,1024]{1,0:T(8,128)S(1)}, u32[]{:S(2)}, u32[]{:S(2)}) collective-permute-start(f32[15,1024]{1,0:T(8,128)S(1)} %get-tuple-element.50), channel_id=1, source_target_pairs={{2,0},{4,2},{6,4},{8,6},{10,8},{12,10},{14,12},{16,14},{18,16},{20... | collective-permute-start | bytes 184328 | tf_op jit(solution)/shard_map/ppermute | solution.py:18
  46.9 8.1 %collective-permute-start.3 = (f32[15,1024]{1,0:T(8,128)S(1)}, f32[15,1024]{1,0:T(8,128)S(1)}, u32[]{:S(2)}, u32[]{:S(2)}) collective-permute-start(f32[15,1024]{1,0:T(8,128)S(1)} %get-tuple-element.51), channel_id=1, source_target_pairs={{0,2},{2,4},{4,6},{6,8},{8,10},{10,12},{12,14},{14,16},{16,18},{18... | collective-permute-start | bytes 184328 | tf_op jit(solution)/shard_map/ppermute | solution.py:15
Sparse Core Ops, SparseCore 0:
  45.7 66.0 all-gather.1
